TPU v7x, 512 devices: a whole 4x8x8 slice. The times are simulated.
512 devices in a mesh: sp: 128 (over z, y, core), tp: 4 (over x).
Axes of the slice: x: 4, y: 8, z: 8, core: 2. Of those that a mesh axis runs over, the one named last changes fastest.
Arguments:
- activations: bfloat16 [65536, 2048], P('sp', 'tp'), may hold values from -250 to 250
- norm_gain: bfloat16 [2048], P('tp'), may hold values from 0.099609375 to 1.8984375
- pool_weight: bfloat16 [2048, 1024], P('sp', 'tp'), may hold values from -0.125 to 0.125
- gate_weight: bfloat16 [2048, 1024], P('sp', 'tp'), may hold values from -0.125 to 0.125
- value_weight: bfloat16 [2048, 1024], P('sp', 'tp'), may hold values from -0.125 to 0.125
- key_weight: bfloat16 [2048, 256], P('sp', 'tp'), may hold values from -0.125 to 0.125
- read_weight: bfloat16 [2048, 256], P('sp', 'tp'), may hold values from -0.125 to 0.125
- step_weight: bfloat16 [2048, 16], P('sp', 'tp'), may hold values from -0.125 to 0.125
- pool_mix: bfloat16 [4, 256, 256], P('tp'), may hold values from -0.375 to 0.375
- pool_scale: float32 [1024], P('tp'), may hold values from 0.1 to 1.9
- taps_value: float32 [4, 1024], P(None, 'tp'), may hold values from -3 to 3
- taps_key: float32 [4, 256], P(None, 'tp'), may hold values from -3 to 3
- taps_read: float32 [4, 256], P(None, 'tp'), may hold values from -3 to 3
- step_bias: float32 [16], P('tp'), may hold values from -1 to 1
- decay_log: float32 [16], P('tp')
- decay_extra: float32 [65536, 16], P('sp', 'tp'), may hold values from -1 to 0
- skip_scale: float32 [16], P('tp'), may hold values from 0.5 to 2
- state_gain: float32 [1024], P('tp'), may hold values from 0.1 to 1.9
- out_pool_weight: bfloat16 [1024, 2048], P('tp', 'sp'), may hold values from -0.125 to 0.125
- out_state_weight: bfloat16 [1024, 2048], P('tp', 'sp'), may hold values from -0.125 to 0.125
Outputs:
- mixed: bfloat16 [65536, 2048], P('sp', 'tp')
All inputs are finite; a program needn't handle non-finite values.
Results may differ from a plain program's by a relative error of at most 0.007.
Values may be sent and summed in bfloat16 or wider, within the bound.
No kernel may reach another device: no remote copies, remote signals or barrier semaphores. Data moves between devices by JAX's collectives and lax.ppermute only.
A program may use at most 64 MiB of HBM per device.

v0:
```python
import jax
import jax.numpy as jnp
from jax import lax
from jax.sharding import Mesh
from jax.sharding import PartitionSpec as P

D = 2048
SSM_STATE = 64
POOL_GROUPS = 4
SCAN_BLOCK = 128
MIX_W = 1024
SP = ("sp_0", "sp_1", "sp_2")
EPSILON = 1e-06
HIGH = lax.Precision.HIGHEST


def sent_to_all(array, axis):
    copies = jnp.broadcast_to(array, (lax.axis_size(axis), *array.shape))
    return lax.all_to_all(copies, axis, split_axis=0, concat_axis=0, tiled=True)


def over_copies(array, axis):
    everything = sent_to_all(array, axis)
    return jnp.sum(everything, axis=0)


def laid_out(pieces, dim):
    pieces = jnp.moveaxis(pieces, 0, dim)
    shape = pieces.shape
    return pieces.reshape(*shape[:dim], shape[dim] * shape[dim + 1], *shape[dim + 2 :])


def collect(array, axis, dim):
    return laid_out(sent_to_all(array, axis), dim)


def shifted(value, axis, steps):
    count = lax.axis_size(axis)
    leading, last = (max(0, -steps), min(count, count - steps))
    return lax.ppermute(value, axis, [(source, source + steps) for source in range(leading, last)])


def neutral_like(array, identity):
    return jax.tree.map(
        lambda part, zero: jnp.zeros_like(part) + jnp.asarray(zero, part.dtype), array, identity
    )


def all_in_one(array, axis):
    leaves = jax.tree.leaves(array)
    order = sorted(range(len(leaves)), key=lambda k: -leaves[k].size)
    width = (1, *leaves[order[0]].shape)[-1]
    lines = [
        jnp.pad(leaves[k].reshape(-1), (0, -leaves[k].size % width)).reshape(-1, width)
        for k in order
    ]
    both, at, found = (lax.all_gather(jnp.concatenate(lines), axis), 0, {})
    for k, line in zip(order, lines):
        section = both[:, at : at + len(line)].reshape(len(both), -1)
        found[k] = section[:, : leaves[k].size].reshape(-1, *leaves[k].shape)
        at += len(line)
    numbers = iter(range(len(leaves)))
    return jax.tree.map(lambda _: found[next(numbers)], array)


def prefix_by_axis(array, axes, combine, identity):
    before = start = neutral_like(array, identity)
    running = array
    for axis in reversed(axes):
        count, place = (lax.axis_size(axis), lax.axis_index(axis))
        pieces = all_in_one(running, axis)
        inside, running = (start, start)
        for k in range(count):
            passed = k < place
            running = combine(running, jax.tree.map(lambda part: part[k], pieces))
            inside = jax.tree.map(lambda new, old: jnp.where(passed, new, old), running, inside)
        before = combine(inside, before)
    return before


def split_up(array, dim, count):
    before, after = (array.shape[:dim], array.shape[dim + 1 :])
    return jnp.moveaxis(array.reshape(*before, count, -1, *after), dim, 0)


def summed_on_arrival(array, axis, dim):
    pieces = split_up(array, dim, lax.axis_size(axis))
    arrived = lax.all_to_all(pieces, axis, split_axis=0, concat_axis=0, tiled=True)
    return arrived.astype(jnp.float32).sum(axis=0)


def backward_kernel(extended, taps):
    width = taps.shape[0]
    length = extended.shape[0] - (width - 1)
    widened_rows = extended.astype(jnp.float32)
    total = jnp.zeros((length, extended.shape[1]), jnp.float32)
    for offset in range(width):
        total = total + taps[offset][None, :] * widened_rows[offset : offset + length]
    return jax.nn.silu(total).astype(jnp.bfloat16)


def combine_states(preceding_token, later):
    return (preceding_token[0] * later[0], preceding_token[1] * later[0][:, None, None] + later[1])


def local(
    activations,
    norm_gain,
    pool_weight,
    gate_weight,
    value_weight,
    key_weight,
    read_weight,
    step_weight,
    pool_mix,
    pool_scale,
    taps_value,
    taps_key,
    taps_read,
    step_bias,
    decay_log,
    decay_extra,
    skip_scale,
    state_gain,
    out_pool_weight,
    out_state_weight,
):
    length = activations.shape[0]
    cluster_span = pool_weight.shape[1]
    local_mix = gate_weight.shape[1]
    local_state = key_weight.shape[1]
    local_heads = step_weight.shape[1]
    joined = jnp.concatenate(
        [pool_weight, gate_weight, value_weight, key_weight, read_weight, step_weight], axis=1
    )
    in_weight = lax.all_gather(joined, SP, axis=0, tiled=True)
    values = activations.astype(jnp.float32)
    squares = over_copies(jnp.sum(values * values, axis=-1), "tp")
    normed = (
        values * lax.rsqrt(squares / D + EPSILON)[:, None] * norm_gain.astype(jnp.float32)
    ).astype(jnp.bfloat16)
    projected = jnp.dot(collect(normed, "tp", 1), in_weight, preferred_element_type=jnp.float32)
    column = 0
    pool_in = projected[:, column : column + cluster_span].astype(jnp.bfloat16)
    column = column + cluster_span
    gate_in = projected[:, column : column + local_mix].astype(jnp.bfloat16)
    column = column + local_mix
    raw_value = projected[:, column : column + local_mix].astype(jnp.bfloat16)
    column = column + local_mix
    raw_key = projected[:, column : column + local_state].astype(jnp.bfloat16)
    column = column + local_state
    raw_read = projected[:, column : column + local_state].astype(jnp.bfloat16)
    column = column + local_state
    step_raw = projected[:, column : column + local_heads]
    raw_joined = jnp.concatenate([raw_value, raw_key, raw_read], axis=1)
    reach = 2**POOL_GROUPS - 1
    width = taps_value.shape[0]
    prior_pool, prior_joined = shifted(
        (pool_in[length - reach :], raw_joined[length - width + 1 :]), SP, 1
    )
    group = lax.axis_index("tp")
    running = jnp.concatenate([prior_pool, pool_in], axis=0).astype(jnp.float32)
    levels = []
    for level in range(POOL_GROUPS):
        stride = 2**level
        running = running[stride:] + running[:-stride]
        levels.append(running[running.shape[0] - length :])
    window_sum = lax.dynamic_index_in_dim(jnp.stack(levels), group, 0, keepdims=False)
    window = jnp.exp2((group + 1).astype(jnp.float32))
    position = (lax.axis_index(SP) * length + jnp.arange(length, dtype=jnp.int32)).astype(
        jnp.float32
    )
    counts = jnp.minimum(position + 1.0, window)
    pooled = (window_sum / counts[:, None] - pool_in.astype(jnp.float32)).astype(jnp.bfloat16)
    pool_out = (
        jnp.dot(pooled, pool_mix[0], preferred_element_type=jnp.float32) * pool_scale
    ).astype(jnp.bfloat16)
    all_taps = jnp.concatenate([taps_value, taps_key, taps_read], axis=1)
    convolved = backward_kernel(jnp.concatenate([prior_joined, raw_joined], axis=0), all_taps)
    head_value = convolved[:, :local_mix]
    key_vectors = convolved[:, local_mix : local_mix + local_state]
    read_vectors = convolved[:, local_mix + local_state :]
    head_dim = local_mix // local_heads
    groups_here = local_state // SSM_STATE
    repeat = local_heads // groups_here
    blocks = length // SCAN_BLOCK
    step_size = jax.nn.softplus(step_raw + step_bias)
    log_decay = -jnp.exp(decay_log) * step_size + decay_extra
    value_heads = head_value.astype(jnp.float32).reshape(length, local_heads, head_dim)
    value_blocks = value_heads.reshape(blocks, SCAN_BLOCK, local_heads, head_dim)
    key_blocks = jnp.repeat(
        key_vectors.astype(jnp.float32).reshape(length, groups_here, SSM_STATE), repeat, axis=1
    ).reshape(blocks, SCAN_BLOCK, local_heads, SSM_STATE)
    read_blocks = jnp.repeat(
        read_vectors.astype(jnp.float32).reshape(length, groups_here, SSM_STATE), repeat, axis=1
    ).reshape(blocks, SCAN_BLOCK, local_heads, SSM_STATE)
    step_blocks = step_size.reshape(blocks, SCAN_BLOCK, local_heads)
    running_decay = jnp.cumsum(log_decay.reshape(blocks, SCAN_BLOCK, local_heads), axis=1)
    lower = jnp.arange(SCAN_BLOCK)[:, None] >= jnp.arange(SCAN_BLOCK)[None, :]
    gaps = jnp.where(
        lower[None, :, :, None],
        running_decay[:, :, None, :] - running_decay[:, None, :, :],
        -jnp.inf,
    )
    weights = jnp.einsum("blhn,bshn->blsh", read_blocks, key_blocks, precision=HIGH) * jnp.exp(gaps)
    scaled_value = value_blocks * step_blocks[..., None]
    inner = jnp.einsum("blsh,bshp->blhp", weights, scaled_value, precision=HIGH)
    block_ends = running_decay[:, -1, :]
    trailing = jnp.exp(block_ends[:, None, :] - running_decay)
    fresh = jnp.einsum("bshn,bsh,bshp->bhpn", key_blocks, trailing, scaled_value, precision=HIGH)

    def advance(carry, inputs):
        block_decay, block_state = inputs
        return (carry * block_decay[:, None, None] + block_state, carry)

    local_total, prefix = lax.scan(
        advance,
        jnp.zeros((local_heads, head_dim, SSM_STATE), jnp.float32),
        (jnp.exp(block_ends), fresh),
    )
    offsets = jnp.cumsum(block_ends, axis=0) - block_ends
    device_decay = jnp.exp(offsets[-1] + block_ends[-1])
    incoming_decay, incoming = prefix_by_axis(
        (device_decay, local_total),
        SP,
        combine_states,
        (jnp.ones_like(device_decay), jnp.zeros_like(local_total)),
    )
    from_device = running_decay + offsets[:, None, :]
    local_off = (
        jnp.einsum("blhn,bhpn->blhp", read_blocks, prefix, precision=HIGH)
        * jnp.exp(running_decay)[..., None]
    )
    far_off = (
        jnp.einsum("blhn,hpn->blhp", read_blocks, incoming, precision=HIGH)
        * jnp.exp(from_device)[..., None]
    )
    scan_out = (inner + local_off + far_off).reshape(length, local_heads, head_dim) + skip_scale[
        None, :, None
    ] * value_heads
    gated = scan_out.reshape(length, local_mix) * jax.nn.silu(gate_in.astype(jnp.float32))
    gate_squares = over_copies(jnp.sum(gated * gated, axis=-1), "tp")
    state_out = (gated * lax.rsqrt(gate_squares / MIX_W + EPSILON)[:, None] * state_gain).astype(
        jnp.bfloat16
    )
    branch_rows = jnp.concatenate([pool_out, state_out], axis=1)
    out_weight = jnp.concatenate([out_pool_weight, out_state_weight], axis=0)
    terms = jnp.dot(
        branch_rows,
        lax.all_gather(out_weight, SP, axis=1, tiled=True),
        preferred_element_type=jnp.float32,
    )
    result = summed_on_arrival(terms.astype(jnp.bfloat16), "tp", 1)
    return result.astype(jnp.bfloat16)


def solution(mesh):
    torus = Mesh(mesh.devices.reshape(8, 8, 2, mesh.shape["tp"]), ("sp_0", "sp_1", "sp_2", "tp"))
    placed = (
        P(SP, "tp"),
        P("tp"),
        P(SP, "tp"),
        P(SP, "tp"),
        P(SP, "tp"),
        P(SP, "tp"),
        P(SP, "tp"),
        P(SP, "tp"),
        P("tp", None, None),
        P("tp"),
        P(None, "tp"),
        P(None, "tp"),
        P(None, "tp"),
        P("tp"),
        P("tp"),
        P(SP, "tp"),
        P("tp"),
        P("tp"),
        P("tp", SP),
        P("tp", SP),
    )
    return jax.shard_map(local, mesh=torus, in_specs=placed, out_specs=P(SP, "tp"), check_vma=False)
```

profile of v0, /device:TPU:24, one launch (start us, length us, event | category | flops | bytes accessed | tf_op | source)
XLA Modules:
  0.0 253.4 jit_solution(12574823793756148212)
XLA Ops:
  10.6 4.3 %all-to-all-start = ((f32[4,1,512]{2,1,0:T(1,128)}), f32[4,1,512]{2,1,0:T(1,128)S(1)}, u32[]{:S(2)}, u32[]{:S(2)}) async-start(f32[4,1,512]{2,1,0:T(1,128)} %broadcast_in_dim.62), calls=%async_computation | async-start | bytes 16384 | tf_op jit(solution)/shard_map/all_to_all | solution.py:19
  15.6 4.6 %all-to-all-done = f32[4,1,512]{2,1,0:T(1,128)S(1)} async-done(((f32[4,1,512]{2,1,0:T(1,128)}), f32[4,1,512]{2,1,0:T(1,128)S(1)}, u32[]{:S(2)}, u32[]{:S(2)}) %all-to-all-start) | async-done | bytes 8224 | tf_op jit(solution)/shard_map/all_to_all | solution.py:19
  21.7 1.6 broadcast_in_dim.63
  23.4 3.8 %all-to-all-start.1 = ((bf16[4,512,512]{1,2,0:T(8,128)(2,1)}), bf16[4,512,512]{1,2,0:T(8,128)(2,1)S(1)}, u32[]{:S(2)}, u32[]{:S(2)}) async-start(bf16[4,512,512]{1,2,0:T(8,128)(2,1)} %broadcast_in_dim.63), calls=%async_computation.1 | async-start | bytes 4194304 | tf_op jit(solution)/shard_map/all_to_all | solution.py:19
  30.6 21.7 %all-to-all-done.1 = bf16[4,512,512]{1,2,0:T(8,128)(2,1)S(1)} async-done(((bf16[4,512,512]{1,2,0:T(8,128)(2,1)}), bf16[4,512,512]{1,2,0:T(8,128)(2,1)S(1)}, u32[]{:S(2)}, u32[]{:S(2)}) %all-to-all-start.1) | async-done | bytes 2097184 | tf_op jit(solution)/shard_map/all_to_all | solution.py:19
  52.3 46.8 %all-gather.9.cloned.1.call-done = bf16[2048,900]{1,0:T(8,128)(2,1)} async-done(((bf16[16,900]{1,0:T(8,128)(2,1)}), bf16[2048,900]{1,0:T(8,128)(2,1)}) %all-gather.9.cloned.1.call-update) | async-done | bytes 3686416 | tf_op jit(solution)/shard_map/all_gather | solution.py:136
  99.1 4.4 %fusion.160 = (bf16[512,900]{0,1:T(8,128)(2,1)S(1)}, f32[512,900]{0,1:T(8,128)S(1)}) fusion(bf16[512,2048]{0,1:T(8,128)(2,1)S(1)} %bitcast.291, bf16[2048,900]{1,0:T(8,128)(2,1)} %all-gather.9.cloned.1.call-done), kind=kOutput, calls=%fused_computation.265 | convolution fusion | flops 1887897600 | bytes 8548352 | tf_op jit(solution)/shard_map/dot_general | solution.py:142
  104.3 2.1 collective-permute-start.1
  109.6 3.6 %collective-permute-start = (bf16[15,256]{0,1:T(8,128)(2,1)}, bf16[15,256]{0,1:T(8,128)(2,1)}, u32[]{:S(2)}, u32[]{:S(2)}) collective-permute-start(bf16[15,256]{0,1:T(8,128)(2,1)} %slice.355), channel_id=1, source_target_pairs={{0,4},{4,8},{8,12},{12,16},{16,20},{20,24},{24,28},{28,32},{32,36}... | collective-permute-start | bytes 23048 | tf_op jit(solution)/shard_map/ppermute | solution.py:40
  116.3 3.1 %while.13 = (s32[]{:T(128)}, f32[4,64,64]{2,1,0:T(8,128)S(1)}, f32[4,4,64,64]{3,2,1,0:T(8,128)}, f32[4,4]{1,0:T(4,128)S(1)}, f32[4,4,64,64]{3,2,1,0:T(8,128)S(1)}, /*index=5*/s32[]{:T(128)}, s32[]{:T(128)}) while((s32[]{:T(128)}, f32[4,64,64]{2,1,0:T(8,128)S(1)}, f32[4,4,64,64]{3,2,1,0:T(8,128)}, f32[4,4]{1,0:T(4,128)S(1)}, ...), condition=%wide.region_4.5_spmd.clone, body=%wide.region_3.4_spmd.clone.sunk | while | flops 65539 | bytes 393872 | solution.py:216
  119.6 1.9 all-gather.3
  122.5 26.2 %all-gather.4 = f32[8,257,64]{1,2,0:T(8,128)S(1)} all-gather(f32[1,257,64]{1,2,0:T(8,128)S(1)} %maximum_bitcast_fusion.1), channel_id=3, replica_groups=mesh['sp_0'=8,'sp_1'=8,'sp_2'=2,'tp'=4] {'sp_1'}, dimensions={0}, use_global_device_ids=true | all-gather | bytes 592128 | tf_op jit(solution)/shard_map/all_gather | solution.py:57
  150.9 27.0 %all-gather.5 = f32[8,257,64]{1,2,0:T(8,128)S(1)} all-gather(f32[1,257,64]{1,2,0:T(8,128)S(1)} %maximum_bitcast_fusion.2), channel_id=4, replica_groups=mesh['sp_0'=8,'sp_1'=8,'sp_2'=2,'tp'=4] {'sp_0'}, dimensions={0}, use_global_device_ids=true | all-gather | bytes 592128 | tf_op jit(solution)/shard_map/all_gather | solution.py:57
  178.7 1.6 copy.267
  180.3 1.6 copy.268
  181.9 1.6 copy.269
  183.5 1.6 copy.270
  185.1 1.6 copy.271
  186.7 1.6 copy.272
  188.3 1.6 copy.273
  192.1 1.6 copy.275
  193.7 1.6 copy.276
  195.3 1.6 copy.277
  198.4 1.6 copy.280
  200.0 1.6 copy.281
  204.0 1.7 fusion.4
  205.7 2.8 %fusion.1 = f32[4,128,128,4]{1,2,3,0:T(8,128)S(1)} fusion(f32[4,128,4]{1,2,0:T(4,128)} %copy.230, pred[128,128]{0,1:T(8,128)(4,1)} %iota_compare_fusion, f32[4,128,64]{1,2,0:T(8,128)S(1)} %bitcast.295, f32[4,128,64]{1,2,0:T(8,128)S(1)} %bitcast.299), kind=kOutput, calls=%fused_computation.11 | convolution fusion | flops 202113024 | bytes 1335296 | tf_op jit(solution)/shard_map/blhn,bshn->blsh/dot_general | solution.py:205
  208.6 2.4 fusion.5
  213.4 4.3 %all-to-all-start.2 = ((f32[4,1,512]{2,1,0:T(1,128)}), f32[4,1,512]{2,1,0:T(1,128)S(1)}, u32[]{:S(2)}, u32[]{:S(2)}) async-start(f32[4,1,512]{2,1,0:T(1,128)} %broadcast_in_dim.73), calls=%async_computation.2 | async-start | bytes 16384 | tf_op jit(solution)/shard_map/all_to_all | solution.py:19
  220.5 2.5 all-to-all-done.2
  223.2 2.9 %convolution_convert_fusion = bf16[512,2048]{1,0:T(8,128)(2,1)S(1)} fusion(bf16[512,2048]{0,1:T(8,128)(2,1)} %all-gather.11.cloned.1.call-done, bf16[512,256]{0,1:T(8,128)(2,1)S(1)} %multiply_convert_fusion.1, bf16[512,256]{0,1:T(8,128)(2,1)S(1)} %fusion.6), kind=kOutput, calls=%fused_computation.4 | convolution fusion | flops 1075838976 | bytes 4718592 | tf_op jit(solution)/shard_map/dot_general | solution.py:248
  226.3 19.0 %all_to_all.22 = bf16[4,512,512]{2,1,0:T(8,128)(2,1)S(1)} all-to-all(bf16[4,512,512]{2,1,0:T(8,128)(2,1)S(1)} %bitcast.290), channel_id=1, replica_groups=mesh['sp_0'=8,'sp_1'=8,'sp_2'=2,'tp'=4] {'tp'}, dimensions={0} | all-to-all | bytes 4194304 | tf_op jit(solution)/shard_map/all_to_all | solution.py:88
  (209 shorter events, 36.2 us)
Async XLA Ops:
  6.5 213.4 %copy-start = (bf16[1,256,256]{2,1,0:T(8,128)(2,1)S(1)}, bf16[1,256,256]{2,1,0:T(8,128)(2,1)}, u32[]{:S(2)}) copy-start(bf16[1,256,256]{2,1,0:T(8,128)(2,1)} %param.30) | copy-start | bytes 393220
  6.5 92.5 %all-gather.9.cloned.1.call-start = ((), (), s32[]{:S(2)}) async-start(), calls=%async_computation.4 | async-start | bytes 4227072 | tf_op jit(solution)/shard_map/all_gather | solution.py:136
  10.6 9.6 %all-to-all-start = ((f32[4,1,512]{2,1,0:T(1,128)}), f32[4,1,512]{2,1,0:T(1,128)S(1)}, u32[]{:S(2)}, u32[]{:S(2)}) async-start(f32[4,1,512]{2,1,0:T(1,128)} %broadcast_in_dim.62), calls=%async_computation | async-start | bytes 16384 | tf_op jit(solution)/shard_map/all_to_all | solution.py:19
  23.3 3.9 %copy-start.15 = (bf16[256,16]{0,1:T(8,128)(2,1)S(1)}, bf16[256,16]{0,1:T(8,128)(2,1)}, u32[]{:S(2)}) copy-start(bf16[256,16]{0,1:T(8,128)(2,1)} %param.41) | copy-start | bytes 24580
  23.3 3.9 %copy-start.16 = (bf16[256,16]{0,1:T(8,128)(2,1)S(1)}, bf16[256,16]{0,1:T(8,128)(2,1)}, u32[]{:S(2)}) copy-start(bf16[256,16]{0,1:T(8,128)(2,1)} %param.40) | copy-start | bytes 24580
  23.3 4.6 %copy-start.36 = (f32[4]{0:T(128)S(1)}, f32[4]{0:T(128)}, u32[]{:S(2)}) copy-start(f32[4]{0:T(128)} %param.38) | copy-start | bytes 52
  23.3 6.0 %copy-start.26 = (f32[4,256]{1,0:T(4,128)S(1)}, f32[4,256]{1,0:T(4,128)}, u32[]{:S(2)}) copy-start(f32[4,256]{1,0:T(4,128)} %param.32) | copy-start | bytes 12292
  23.3 6.0 %copy-start.30 = (f32[4,64]{1,0:T(4,128)S(1)}, f32[4,64]{1,0:T(4,128)}, u32[]{:S(2)}) copy-start(f32[4,64]{1,0:T(4,128)} %param.34) | copy-start | bytes 3076
  23.3 5.9 %copy-start.31 = (f32[4,64]{1,0:T(4,128)S(1)}, f32[4,64]{1,0:T(4,128)}, u32[]{:S(2)}) copy-start(f32[4,64]{1,0:T(4,128)} %param.33) | copy-start | bytes 3076
  23.3 7.2 %copy-start.38 = (f32[4]{0:T(128)S(1)}, f32[4]{0:T(128)}, u32[]{:S(2)}) copy-start(f32[4]{0:T(128)} %param.36) | copy-start | bytes 52
  23.4 28.9 %all-to-all-start.1 = ((bf16[4,512,512]{1,2,0:T(8,128)(2,1)}), bf16[4,512,512]{1,2,0:T(8,128)(2,1)S(1)}, u32[]{:S(2)}, u32[]{:S(2)}) async-start(bf16[4,512,512]{1,2,0:T(8,128)(2,1)} %broadcast_in_dim.63), calls=%async_computation.1 | async-start | bytes 4194304 | tf_op jit(solution)/shard_map/all_to_all | solution.py:19
  27.1 196.1 %all-gather.11.cloned.1.call-start = ((), (), s32[]{:S(2)}) async-start(), calls=%async_computation.5 | async-start | bytes 2113536 | tf_op jit(solution)/shard_map/all_gather | solution.py:250
  99.1 4.4 %copy-start.17 = (f32[512,4]{0,1:T(4,128)S(1)}, f32[512,4]{0,1:T(4,128)}, u32[]{:S(2)}) copy-start(f32[512,4]{0,1:T(4,128)} %param.37) | copy-start | bytes 24580
  99.1 4.4 %copy-start.35 = (f32[4]{0:T(128)S(1)}, f32[4]{0:T(128)}, u32[]{:S(2)}) copy-start(f32[4]{0:T(128)} %param.35) | copy-start | bytes 52
  104.2 9.2 %copy-start.11 = (f32[384]{0:T(512)S(1)}, f32[384]{0:T(512)}, u32[]{:S(2)}) copy-start(f32[384]{0:T(512)} %get-tuple-element.53) | copy-start | bytes 4612
  104.2 9.2 %copy-start.12 = (f32[384]{0:T(512)S(1)}, f32[384]{0:T(512)}, u32[]{:S(2)}) copy-start(f32[384]{0:T(512)} %get-tuple-element.54) | copy-start | bytes 4612
  104.2 9.2 %copy-start.13 = (f32[384]{0:T(512)S(1)}, f32[384]{0:T(512)}, u32[]{:S(2)}) copy-start(f32[384]{0:T(512)} %get-tuple-element.55) | copy-start | bytes 4612
  104.2 9.2 %copy-start.14 = (f32[384]{0:T(512)S(1)}, f32[384]{0:T(512)}, u32[]{:S(2)}) copy-start(f32[384]{0:T(512)} %get-tuple-element.56) | copy-start | bytes 4612
  104.3 8.9 %collective-permute-start.1 = (bf16[3,384]{0,1:T(8,128)(2,1)S(1)}, bf16[3,384]{0,1:T(8,128)(2,1)S(1)}, u32[]{:S(2)}, u32[]{:S(2)}) collective-permute-start(bf16[3,384]{0,1:T(8,128)(2,1)S(1)} %slice.368), channel_id=1, source_target_pairs={{0,4},{4,8},{8,12},{12,16},{16,20},{20,24},{24,28},{28,32},{32,36}... | collective-permute-start | bytes 6920 | tf_op jit(solution)/shard_map/ppermute | solution.py:40
  109.6 108.1 %collective-permute-start = (bf16[15,256]{0,1:T(8,128)(2,1)}, bf16[15,256]{0,1:T(8,128)(2,1)}, u32[]{:S(2)}, u32[]{:S(2)}) collective-permute-start(bf16[15,256]{0,1:T(8,128)(2,1)} %slice.355), channel_id=1, source_target_pairs={{0,4},{4,8},{8,12},{12,16},{16,20},{20,24},{24,28},{28,32},{32,36}... | collective-permute-start | bytes 23048 | tf_op jit(solution)/shard_map/ppermute | solution.py:40
  121.6 27.2 %copy-start.25 = (f32[4]{0:T(128)}, f32[4]{0:T(128)S(1)}, u32[]{:S(2)}) copy-start(f32[4]{0:T(128)S(1)} %get-tuple-element.116) | copy-start | bytes 52
  121.6 27.2 %copy-start.33 = (f32[4]{0:T(128)}, f32[4]{0:T(128)S(1)}, u32[]{:S(2)}) copy-start(f32[4]{0:T(128)S(1)} %get-tuple-element.117) | copy-start | bytes 52
  191.3 12.6 %copy-start.3 = (f32[8,4,8,128]{3,2,1,0:T(8,128)S(1)}, f32[8,4,8,128]{3,2,1,0:T(8,128)}, u32[]{:S(2)}) copy-start(f32[8,4,8,128]{3,2,1,0:T(8,128)} %get-tuple-element.93) | copy-start | bytes 393220
  192.1 11.9 %copy-start.10 = (f32[8,1,64]{2,0,1:T(8,128)S(1)}, f32[8,1,64]{2,0,1:T(8,128)}, u32[]{:S(2)}) copy-start(f32[8,1,64]{2,0,1:T(8,128)} %copy.288) | copy-start | bytes 6148
  192.1 13.6 %copy-start.2 = (f32[8,4,8,128]{3,2,0,1:T(8,128)S(1)}, f32[8,4,8,128]{3,2,0,1:T(8,128)}, u32[]{:S(2)}) copy-start(f32[8,4,8,128]{3,2,0,1:T(8,128)} %copy-done.1) | copy-start | bytes 393220
  198.4 10.1 %copy-start.4 = (f32[1,256,64]{2,1,0:T(8,128)S(1)}, f32[1,256,64]{2,1,0:T(8,128)}, u32[]{:S(2)}) copy-start(f32[1,256,64]{2,1,0:T(8,128)} %copy.267) | copy-start | bytes 196612
  202.4 6.1 %copy-start.5 = (f32[1,256,64]{2,1,0:T(8,128)S(1)}, f32[1,256,64]{2,1,0:T(8,128)}, u32[]{:S(2)}) copy-start(f32[1,256,64]{2,1,0:T(8,128)} %copy.280) | copy-start | bytes 196612
  203.9 4.6 %copy-start.6 = (f32[1,256,64]{2,1,0:T(8,128)S(1)}, f32[1,256,64]{2,1,0:T(8,128)}, u32[]{:S(2)}) copy-start(f32[1,256,64]{2,1,0:T(8,128)} %copy.281) | copy-start | bytes 196612
  203.9 4.6 %copy-start.7 = (f32[1,256,64]{2,1,0:T(8,128)S(1)}, f32[1,256,64]{2,1,0:T(8,128)}, u32[]{:S(2)}) copy-start(f32[1,256,64]{2,1,0:T(8,128)} %copy.282) | copy-start | bytes 196612
  203.9 4.6 %copy-start.8 = (f32[1,256,64]{2,1,0:T(8,128)S(1)}, f32[1,256,64]{2,1,0:T(8,128)}, u32[]{:S(2)}) copy-start(f32[1,256,64]{2,1,0:T(8,128)} %copy.283) | copy-start | bytes 196612
  203.9 4.7 %copy-start.9 = (f32[1,256,64]{2,1,0:T(8,128)S(1)}, f32[1,256,64]{2,1,0:T(8,128)}, u32[]{:S(2)}) copy-start(f32[1,256,64]{2,1,0:T(8,128)} %copy.284) | copy-start | bytes 196612
  213.4 9.7 %all-to-all-start.2 = ((f32[4,1,512]{2,1,0:T(1,128)}), f32[4,1,512]{2,1,0:T(1,128)S(1)}, u32[]{:S(2)}, u32[]{:S(2)}) async-start(f32[4,1,512]{2,1,0:T(1,128)} %broadcast_in_dim.73), calls=%async_computation.2 | async-start | bytes 16384 | tf_op jit(solution)/shard_map/all_to_all | solution.py:19
  (14 other events, 22.8 us)
Sparse Core Ops, SparseCore 0:
  10.5 88.5 all-gather.8
  102.2 80.5 all-gather.10
where the time goes:
time: 255 us; the launch traced here: 253 us
  waiting for transfers between devices  75.8 us (30%)
  blocking collectives  74.1 us (29%)
  local copies, waits for them, and re-layouts  39.7 us (16%)
  starting transfers between devices  18.1 us (7%)
  matrix products  16.7 us (7%)
  other arithmetic  14.6 us (6%)
  between operations  14.4 us (6%)
    all_gather x3, blocking collectives, all_in_one(): both, at, found = (lax.all_gather(jnp.concatenate(lines), axis), 0, {})  55.1 us
    all_gather x1, waiting for transfers between devices, local(): in_weight = lax.all_gather(joined, SP, axis=0, tiled=True)  46.8 us
    all_to_all x3, waiting for transfers between devices, sent_to_all(): return lax.all_to_all(copies, axis, split_axis=0, concat_axis=0, tiled=True)  28.8 us
    squeeze x18, local copies, waits for them, and re-layouts, prefix_by_axis(): running = combine(running, jax.tree.map(lambda part: part[k], pieces))  23.7 us
    all_to_all x1, blocking collectives, summed_on_arrival(): lax.all_to_all(pieces, axis, split_axis=0, concat_axis=0, tiled=True)  19 us
    all_to_all x3, starting transfers between devices, sent_to_all(): return lax.all_to_all(copies, axis, split_axis=0, concat_axis=0, tiled=True)  12.3 us
    ppermute x2, starting transfers between devices, shifted(): lax.ppermute(value, axis, [(source, source + steps) for source in range(l...  5.72 us
  transfers between devices with their start and end apart: 7, of which 4 were waited for; matrix products, arithmetic and copies ran while one was open for 25% of the time, Pallas kernels for 0%

commit v1 on v0

--- a/solution.py
+++ b/solution.py
@@ -133,7 +133,9 @@
     joined = jnp.concatenate(
         [pool_weight, gate_weight, value_weight, key_weight, read_weight, step_weight], axis=1
     )
-    in_weight = lax.all_gather(joined, SP, axis=0, tiled=True)
+    in_weight = jnp.concatenate(
+        lax.all_to_all(jnp.stack([joined] * lax.axis_size(SP)), SP, 0, 0), axis=0
+    )
     values = activations.astype(jnp.float32)
     squares = over_copies(jnp.sum(values * values, axis=-1), "tp")
     normed = (

time: 255 us -> 329 us (1.29)
  the two profiles are of different devices: /device:TPU:24 before, /device:TPU:2 now
where the time goes in v1:
time: 329 us; the launch traced here: 327 us
  waiting for transfers between devices  117 us (36%)
  blocking collectives  77.1 us (23%)
  starting transfers between devices  46.5 us (14%)
  local copies, waits for them, and re-layouts  41.7 us (13%)
  other arithmetic  15.7 us (5%)
  matrix products  14.7 us (4%)
  between operations  14.7 us (4%)
    all_to_all x1, waiting for transfers between devices, local(): lax.all_to_all(jnp.stack([joined] * lax.axis_size(SP)), SP, 0, 0)  93.2 us
    all_gather x3, blocking collectives, all_in_one(): both, at, found = (lax.all_gather(jnp.concatenate(lines), axis), 0, {})  58.1 us
    squeeze x18, local copies, waits for them, and re-layouts, prefix_by_axis(): running = combine(running, jax.tree.map(lambda part: part[k], pieces))  24.6 us
    all_to_all x3, waiting for transfers between devices, sent_to_all(): return lax.all_to_all(copies, axis, split_axis=0, concat_axis=0, tiled=True)  23.5 us
    all_to_all x3, starting transfers between devices, sent_to_all(): return lax.all_to_all(copies, axis, split_axis=0, concat_axis=0, tiled=True)  20 us
    all_to_all x1, blocking collectives, summed_on_arrival(): lax.all_to_all(pieces, axis, split_axis=0, concat_axis=0, tiled=True)  19 us
    all_to_all x1, starting transfers between devices, local(): lax.all_to_all(jnp.stack([joined] * lax.axis_size(SP)), SP, 0, 0)  18.5 us
    ppermute x2, starting transfers between devices, shifted(): lax.ppermute(value, axis, [(source, source + steps) for source in range(l...  8.01 us
  transfers between devices with their start and end apart: 7, of which 4 were waited for; matrix products, arithmetic and copies ran while one was open for 18% of the time, Pallas kernels for 0%

profile of v1, /device:TPU:2, one launch (start us, length us, event | category | flops | bytes accessed | tf_op | source)
XLA Modules:
  0.0 327.3 jit_solution(6353807504458310868)
XLA Ops:
  8.4 9.1 %all-to-all-start = ((f32[4,1,512]{2,1,0:T(1,128)}), f32[4,1,512]{2,1,0:T(1,128)S(1)}, u32[]{:S(2)}, u32[]{:S(2)}) async-start(f32[4,1,512]{2,1,0:T(1,128)} %broadcast_in_dim.62), calls=%async_computation | async-start | bytes 16384 | tf_op jit(solution)/shard_map/all_to_all | solution.py:19
  18.2 3.2 all-to-all-done
  22.8 1.5 broadcast_in_dim.63
  24.4 5.2 %all-to-all-start.1 = ((bf16[4,512,512]{1,2,0:T(8,128)(2,1)}), bf16[4,512,512]{1,2,0:T(8,128)(2,1)S(1)}, u32[]{:S(2)}, u32[]{:S(2)}) async-start(bf16[4,512,512]{1,2,0:T(8,128)(2,1)} %broadcast_in_dim.63), calls=%async_computation.1 | async-start | bytes 4194304 | tf_op jit(solution)/shard_map/all_to_all | solution.py:19
  29.8 19.2 %all-to-all-done.1 = bf16[4,512,512]{1,2,0:T(8,128)(2,1)S(1)} async-done(((bf16[4,512,512]{1,2,0:T(8,128)(2,1)}), bf16[4,512,512]{1,2,0:T(8,128)(2,1)S(1)}, u32[]{:S(2)}, u32[]{:S(2)}) %all-to-all-start.1) | async-done | bytes 2097184 | tf_op jit(solution)/shard_map/all_to_all | solution.py:19
  49.0 2.5 stack.12
  51.6 18.5 %all-to-all-start.2 = ((bf16[128,16,900]{2,1,0:T(8,128)(2,1)}), bf16[128,16,900]{2,1,0:T(8,128)(2,1)}, u32[]{:S(2)}, u32[]{:S(2)}) async-start(bf16[128,16,900]{2,1,0:T(8,128)(2,1)} %stack.12), calls=%async_computation.2 | async-start | bytes 8388608 | tf_op jit(solution)/shard_map/all_to_all | solution.py:137
  73.6 93.2 %all-to-all-done.2 = bf16[128,16,900]{2,1,0:T(8,128)(2,1)} async-done(((bf16[128,16,900]{2,1,0:T(8,128)(2,1)}), bf16[128,16,900]{2,1,0:T(8,128)(2,1)}, u32[]{:S(2)}, u32[]{:S(2)}) %all-to-all-start.2) | async-done | bytes 3686432 | tf_op jit(solution)/shard_map/all_to_all | solution.py:137
  166.8 4.4 %fusion.160 = (bf16[512,900]{0,1:T(8,128)(2,1)S(1)}, f32[512,900]{0,1:T(8,128)S(1)}) fusion(bf16[512,2048]{0,1:T(8,128)(2,1)S(1)} %bitcast.292, bf16[2048,900]{1,0:T(8,128)(2,1)} %bitcast.2), kind=kOutput, calls=%fused_computation.265 | convolution fusion | flops 1887897600 | bytes 8548352 | tf_op jit(solution)/shard_map/dot_general | solution.py:144
  172.0 1.3 collective-permute-start.1
  176.5 6.7 %collective-permute-start = (bf16[15,256]{0,1:T(8,128)(2,1)}, bf16[15,256]{0,1:T(8,128)(2,1)}, u32[]{:S(2)}, u32[]{:S(2)}) collective-permute-start(bf16[15,256]{0,1:T(8,128)(2,1)} %slice.355), channel_id=1, source_target_pairs={{0,4},{4,8},{8,12},{12,16},{16,20},{20,24},{24,28},{28,32},{32,36}... | collective-permute-start | bytes 23048 | tf_op jit(solution)/shard_map/ppermute | solution.py:40
  186.3 3.1 while.13
  189.6 1.9 all-gather.3
  192.4 27.9 %all-gather.4 = f32[8,257,64]{1,2,0:T(8,128)S(1)} all-gather(f32[1,257,64]{1,2,0:T(8,128)S(1)} %maximum_bitcast_fusion.1), channel_id=3, replica_groups=mesh['sp_0'=8,'sp_1'=8,'sp_2'=2,'tp'=4] {'sp_1'}, dimensions={0}, use_global_device_ids=true | all-gather | bytes 592128 | tf_op jit(solution)/shard_map/all_gather | solution.py:57
  222.6 28.2 %all-gather.5 = f32[8,257,64]{1,2,0:T(8,128)S(1)} all-gather(f32[1,257,64]{1,2,0:T(8,128)S(1)} %maximum_bitcast_fusion.2), channel_id=4, replica_groups=mesh['sp_0'=8,'sp_1'=8,'sp_2'=2,'tp'=4] {'sp_0'}, dimensions={0}, use_global_device_ids=true | all-gather | bytes 592128 | tf_op jit(solution)/shard_map/all_gather | solution.py:57
  251.7 1.6 copy.267
  253.3 1.6 copy.268
  254.9 1.6 copy.269
  256.5 1.6 copy.270
  258.1 1.6 copy.271
  259.7 1.6 copy.272
  261.3 1.6 copy.273
  265.1 1.7 copy.275
  266.8 1.6 copy.276
  268.3 1.6 copy.277
  271.4 1.6 copy.280
  273.1 1.6 copy.281
  276.1 1.6 copy.283
  281.0 2.8 fusion.1
  287.3 5.7 %all-to-all-start.3 = ((f32[4,1,512]{2,1,0:T(1,128)}), f32[4,1,512]{2,1,0:T(1,128)S(1)}, u32[]{:S(2)}, u32[]{:S(2)}) async-start(f32[4,1,512]{2,1,0:T(1,128)} %broadcast_in_dim.73), calls=%async_computation.3 | async-start | bytes 16384 | tf_op jit(solution)/shard_map/all_to_all | solution.py:19
  297.1 2.9 convolution_convert_fusion
  300.2 19.0 %all_to_all.27 = bf16[4,512,512]{2,1,0:T(8,128)(2,1)S(1)} all-to-all(bf16[4,512,512]{2,1,0:T(8,128)(2,1)S(1)} %bitcast.291), channel_id=1, replica_groups=mesh['sp_0'=8,'sp_1'=8,'sp_2'=2,'tp'=4] {'tp'}, dimensions={0} | all-to-all | bytes 4194304 | tf_op jit(solution)/shard_map/all_to_all | solution.py:88
  (271 shorter events, 38.3 us)
Async XLA Ops:
  6.5 288.8 %copy-start = (bf16[1,256,256]{2,1,0:T(8,128)(2,1)S(1)}, bf16[1,256,256]{2,1,0:T(8,128)(2,1)}, u32[]{:S(2)}) copy-start(bf16[1,256,256]{2,1,0:T(8,128)(2,1)} %param.30) | copy-start | bytes 393220
  8.4 13.0 %all-to-all-start = ((f32[4,1,512]{2,1,0:T(1,128)}), f32[4,1,512]{2,1,0:T(1,128)S(1)}, u32[]{:S(2)}, u32[]{:S(2)}) async-start(f32[4,1,512]{2,1,0:T(1,128)} %broadcast_in_dim.62), calls=%async_computation | async-start | bytes 16384 | tf_op jit(solution)/shard_map/all_to_all | solution.py:19
  24.4 24.6 %all-to-all-start.1 = ((bf16[4,512,512]{1,2,0:T(8,128)(2,1)}), bf16[4,512,512]{1,2,0:T(8,128)(2,1)S(1)}, u32[]{:S(2)}, u32[]{:S(2)}) async-start(bf16[4,512,512]{1,2,0:T(8,128)(2,1)} %broadcast_in_dim.63), calls=%async_computation.1 | async-start | bytes 4194304 | tf_op jit(solution)/shard_map/all_to_all | solution.py:19
  51.6 18.6 %copy-start.31 = (bf16[256,16]{0,1:T(8,128)(2,1)S(1)}, bf16[256,16]{0,1:T(8,128)(2,1)}, u32[]{:S(2)}) copy-start(bf16[256,16]{0,1:T(8,128)(2,1)} %param.41) | copy-start | bytes 24580
  51.6 18.6 %copy-start.32 = (bf16[256,16]{0,1:T(8,128)(2,1)S(1)}, bf16[256,16]{0,1:T(8,128)(2,1)}, u32[]{:S(2)}) copy-start(bf16[256,16]{0,1:T(8,128)(2,1)} %param.40) | copy-start | bytes 24580
  51.6 19.3 %copy-start.67 = (f32[4]{0:T(128)S(1)}, f32[4]{0:T(128)}, u32[]{:S(2)}) copy-start(f32[4]{0:T(128)} %param.38) | copy-start | bytes 52
  51.6 20.7 %copy-start.52 = (f32[4,256]{1,0:T(4,128)S(1)}, f32[4,256]{1,0:T(4,128)}, u32[]{:S(2)}) copy-start(f32[4,256]{1,0:T(4,128)} %param.32) | copy-start | bytes 12292
  51.6 20.7 %copy-start.60 = (f32[4,64]{1,0:T(4,128)S(1)}, f32[4,64]{1,0:T(4,128)}, u32[]{:S(2)}) copy-start(f32[4,64]{1,0:T(4,128)} %param.34) | copy-start | bytes 3076
  51.6 20.7 %copy-start.61 = (f32[4,64]{1,0:T(4,128)S(1)}, f32[4,64]{1,0:T(4,128)}, u32[]{:S(2)}) copy-start(f32[4,64]{1,0:T(4,128)} %param.33) | copy-start | bytes 3076
  51.6 22.0 %copy-start.69 = (f32[4]{0:T(128)S(1)}, f32[4]{0:T(128)}, u32[]{:S(2)}) copy-start(f32[4]{0:T(128)} %param.36) | copy-start | bytes 52
  51.6 115.2 %all-to-all-start.2 = ((bf16[128,16,900]{2,1,0:T(8,128)(2,1)}), bf16[128,16,900]{2,1,0:T(8,128)(2,1)}, u32[]{:S(2)}, u32[]{:S(2)}) async-start(bf16[128,16,900]{2,1,0:T(8,128)(2,1)} %stack.12), calls=%async_computation.2 | async-start | bytes 8388608 | tf_op jit(solution)/shard_map/all_to_all | solution.py:137
  70.1 227.0 %all-gather.8.cloned.1.call-start = ((), (), s32[]{:S(2)}) async-start(), calls=%async_computation.5 | async-start | bytes 2113536 | tf_op jit(solution)/shard_map/all_gather | solution.py:252
  171.9 11.5 %copy-start.24 = (f32[384]{0:T(512)S(1)}, f32[384]{0:T(512)}, u32[]{:S(2)}) copy-start(f32[384]{0:T(512)} %get-tuple-element.53) | copy-start | bytes 4612
  171.9 11.5 %copy-start.25 = (f32[384]{0:T(512)S(1)}, f32[384]{0:T(512)}, u32[]{:S(2)}) copy-start(f32[384]{0:T(512)} %get-tuple-element.54) | copy-start | bytes 4612
  171.9 11.5 %copy-start.26 = (f32[384]{0:T(512)S(1)}, f32[384]{0:T(512)}, u32[]{:S(2)}) copy-start(f32[384]{0:T(512)} %get-tuple-element.55) | copy-start | bytes 4612
  171.9 11.5 %copy-start.27 = (f32[384]{0:T(512)S(1)}, f32[384]{0:T(512)}, u32[]{:S(2)}) copy-start(f32[384]{0:T(512)} %get-tuple-element.56) | copy-start | bytes 4612
  172.0 11.2 %collective-permute-start.1 = (bf16[3,384]{0,1:T(8,128)(2,1)S(1)}, bf16[3,384]{0,1:T(8,128)(2,1)S(1)}, u32[]{:S(2)}, u32[]{:S(2)}) collective-permute-start(bf16[3,384]{0,1:T(8,128)(2,1)S(1)} %slice.368), channel_id=1, source_target_pairs={{0,4},{4,8},{8,12},{12,16},{16,20},{20,24},{24,28},{28,32},{32,36}... | collective-permute-start | bytes 6920 | tf_op jit(solution)/shard_map/ppermute | solution.py:40
  176.5 116.6 %collective-permute-start = (bf16[15,256]{0,1:T(8,128)(2,1)}, bf16[15,256]{0,1:T(8,128)(2,1)}, u32[]{:S(2)}, u32[]{:S(2)}) collective-permute-start(bf16[15,256]{0,1:T(8,128)(2,1)} %slice.355), channel_id=1, source_target_pairs={{0,4},{4,8},{8,12},{12,16},{16,20},{20,24},{24,28},{28,32},{32,36}... | collective-permute-start | bytes 23048 | tf_op jit(solution)/shard_map/ppermute | solution.py:40
  191.6 28.9 %copy-start.48 = (f32[4]{0:T(128)}, f32[4]{0:T(128)S(1)}, u32[]{:S(2)}) copy-start(f32[4]{0:T(128)S(1)} %get-tuple-element.116) | copy-start | bytes 52
  191.6 28.9 %copy-start.63 = (f32[4]{0:T(128)}, f32[4]{0:T(128)S(1)}, u32[]{:S(2)}) copy-start(f32[4]{0:T(128)S(1)} %get-tuple-element.117) | copy-start | bytes 52
  264.3 14.3 %copy-start.4 = (f32[8,4,8,128]{3,2,1,0:T(8,128)S(1)}, f32[8,4,8,128]{3,2,1,0:T(8,128)}, u32[]{:S(2)}) copy-start(f32[8,4,8,128]{3,2,1,0:T(8,128)} %get-tuple-element.93) | copy-start | bytes 393220
  265.1 14.6 %copy-start.1 = (f32[4,4,64,64]{3,2,1,0:T(8,128)S(1)}, f32[4,4,64,64]{3,2,1,0:T(8,128)}, u32[]{:S(2)}) copy-start(f32[4,4,64,64]{3,2,1,0:T(8,128)} %get-tuple-element.33) | copy-start | bytes 786436
  265.1 15.9 %copy-start.3 = (f32[8,4,8,128]{3,2,0,1:T(8,128)S(1)}, f32[8,4,8,128]{3,2,0,1:T(8,128)}, u32[]{:S(2)}) copy-start(f32[8,4,8,128]{3,2,0,1:T(8,128)} %copy-done.2) | copy-start | bytes 393220
  271.4 12.3 %copy-start.5 = (f32[1,256,64]{2,1,0:T(8,128)S(1)}, f32[1,256,64]{2,1,0:T(8,128)}, u32[]{:S(2)}) copy-start(f32[1,256,64]{2,1,0:T(8,128)} %copy.267) | copy-start | bytes 196612
  271.4 12.3 %copy-start.6 = (f32[1,256,64]{2,1,0:T(8,128)S(1)}, f32[1,256,64]{2,1,0:T(8,128)}, u32[]{:S(2)}) copy-start(f32[1,256,64]{2,1,0:T(8,128)} %copy.268) | copy-start | bytes 196612
  276.1 7.8 %copy-start.41 = (f32[4]{0:T(128)S(1)}, f32[4]{0:T(128)}, u32[]{:S(2)}) copy-start(f32[4]{0:T(128)} %copy-done.40) | copy-start | bytes 52
  276.1 7.8 %copy-start.43 = (f32[4]{0:T(128)S(1)}, f32[4]{0:T(128)}, u32[]{:S(2)}) copy-start(f32[4]{0:T(128)} %copy-done.42) | copy-start | bytes 52
  276.1 7.8 %copy-start.45 = (f32[4]{0:T(128)S(1)}, f32[4]{0:T(128)}, u32[]{:S(2)}) copy-start(f32[4]{0:T(128)} %copy-done.44) | copy-start | bytes 52
  276.1 7.8 %copy-start.47 = (f32[4]{0:T(128)S(1)}, f32[4]{0:T(128)}, u32[]{:S(2)}) copy-start(f32[4]{0:T(128)} %copy-done.46) | copy-start | bytes 52
  276.1 7.8 %copy-start.49 = (f32[4]{0:T(128)S(1)}, f32[4]{0:T(128)}, u32[]{:S(2)}) copy-start(f32[4]{0:T(128)} %copy-done.48) | copy-start | bytes 52
  276.1 7.8 %copy-start.55 = (f32[4]{0:T(128)S(1)}, f32[4]{0:T(128)}, u32[]{:S(2)}) copy-start(f32[4]{0:T(128)} %copy-done.54) | copy-start | bytes 52
  287.3 9.6 %all-to-all-start.3 = ((f32[4,1,512]{2,1,0:T(1,128)}), f32[4,1,512]{2,1,0:T(1,128)S(1)}, u32[]{:S(2)}, u32[]{:S(2)}) async-start(f32[4,1,512]{2,1,0:T(1,128)} %broadcast_in_dim.73), calls=%async_computation.3 | async-start | bytes 16384 | tf_op jit(solution)/shard_map/all_to_all | solution.py:19
  (45 other events, 203.0 us)
Sparse Core Ops, SparseCore 0:
  74.0 150.9 all-gather.7
